TPU v7x, 32 devices: a whole 2x2x4 slice. The times are simulated.
32 devices in a mesh: sp: 4 (over y, x), tp: 8 (over z, core).
Axes of the slice: x: 2, y: 2, z: 4, core: 2. Of those that a mesh axis runs over, the one named last changes fastest.
Arguments:
- tokens: bfloat16 [2048, 4096], P('sp', 'tp'), may hold values from -6 to 6
- pre_gain: float32 [2, 4096], replicated, may hold values from 0.1 to 1.9
- w_value: bfloat16 [2, 4096, 4096], P(None, 'sp', 'tp'), may hold values from -0.09375 to 0.09375
- w_gate: bfloat16 [2, 4096, 4096], P(None, 'sp', 'tp'), may hold values from -0.09375 to 0.09375
- conv_taps: float32 [2, 31, 4096], P(None, None, 'tp'), may hold values from -3.5 to 3.5
- conv_bias: float32 [2, 4096], P(None, 'tp'), may hold values from -3 to 3
- norm_gain: float32 [2, 4096], P(None, 'tp'), may hold values from 0.1 to 1.9
- norm_bias: float32 [2, 4096], P(None, 'tp'), may hold values from -3 to 3
- w_out: bfloat16 [2, 4096, 4096], P(None, 'sp', 'tp'), may hold values from -0.09375 to 0.09375
- post_gain: float32 [2, 4096], P(None, 'tp'), may hold values from 0.1 to 1.9
Outputs:
- stream: bfloat16 [2048, 4096], P('sp', 'tp')
All inputs are finite; a program needn't handle non-finite values.
Results may differ from a plain program's by a relative error of at most 0.009.
Values may be sent and summed in bfloat16 or wider, within the bound.
A program may use at most 64 MiB of HBM per device.

v0:
```python
import jax
import jax.numpy as jnp
from jax import lax
from jax.sharding import PartitionSpec as P


def passed_along(value, axis, steps):
    count = lax.axis_size(axis)
    leading, last = (max(0, -steps), min(count, count - steps))
    return lax.ppermute(value, axis, [(source, source + steps) for source in range(leading, last)])


def shards(
    tokens, pre_gain, w_value, w_gate, conv_taps, conv_bias, norm_gain, norm_bias, w_out, post_gain
):
    layer_count = w_value.shape[0]
    tap_count = conv_taps.shape[1]
    channel_count = conv_taps.shape[2] * lax.axis_size("tp")
    model_width = tokens.shape[1] * lax.axis_size("tp")
    local_rows = tokens.shape[0]
    every_value, every_gate, every_out = (
        lax.all_gather(w_value, "sp", axis=1, tiled=True),
        lax.all_gather(w_gate, "sp", axis=1, tiled=True),
        lax.all_gather(w_out, "sp", axis=1, tiled=True),
    )
    stream = tokens
    for layer_index in range(layer_count):
        gathered = lax.all_gather(stream, "tp", axis=1, tiled=True)
        full_rows = gathered.astype(jnp.float32)
        scale_rows = lax.rsqrt(jnp.mean(full_rows * full_rows, axis=-1, keepdims=True) + 1e-06)
        normed = (full_rows * scale_rows * pre_gain[layer_index]).astype(jnp.bfloat16)
        value_block = every_value[layer_index]
        gate_block = every_gate[layer_index]
        out_block = every_out[layer_index]
        value_proj = jnp.dot(normed, value_block, preferred_element_type=jnp.float32)
        gate_proj = jnp.dot(normed, gate_block, preferred_element_type=jnp.float32)
        glu_out = (value_proj * jax.nn.sigmoid(gate_proj)).astype(jnp.bfloat16)
        earlier = passed_along(glu_out[local_rows - (tap_count - 1) :], "sp", 1)
        padded = jnp.concatenate([earlier, glu_out], axis=0).astype(jnp.float32)
        filtered = jnp.zeros(glu_out.shape, jnp.float32) + conv_bias[layer_index]
        for tap_index in range(tap_count):
            filtered = (
                filtered
                + padded[tap_index : tap_index + local_rows] * conv_taps[layer_index, tap_index]
            )
        channel_sum, channel_square = lax.psum(
            (jnp.sum(filtered, axis=-1), jnp.sum(filtered * filtered, axis=-1)), "tp"
        )
        centre = channel_sum / channel_count
        spread = jnp.maximum(channel_square / channel_count - centre * centre, 0.0)
        shaped = (filtered - centre[:, None]) * lax.rsqrt(spread + 1e-05)[:, None]
        mixed = jax.nn.silu(shaped * norm_gain[layer_index] + norm_bias[layer_index]).astype(
            jnp.bfloat16
        )
        whole_mixed = lax.all_gather(mixed, "tp", axis=1, tiled=True)
        branch_low = jnp.dot(whole_mixed, out_block, preferred_element_type=jnp.float32).astype(
            jnp.bfloat16
        )
        branch = lax.optimization_barrier(branch_low).astype(jnp.float32)
        total = lax.psum(jnp.sum(branch * branch, axis=-1), "tp")
        rescale = lax.rsqrt(total / model_width + 1e-06)[:, None]
        stream = (stream.astype(jnp.float32) + branch * rescale * post_gain[layer_index]).astype(
            jnp.bfloat16
        )
    return stream


def solution(mesh):
    in_specs = (
        P("sp", "tp"),
        P(),
        P(None, "sp", "tp"),
        P(None, "sp", "tp"),
        P(None, None, "tp"),
        P(None, "tp"),
        P(None, "tp"),
        P(None, "tp"),
        P(None, "sp", "tp"),
        P(None, "tp"),
    )
    out_specs = P("sp", "tp")
    return jax.shard_map(shards, mesh=mesh, in_specs=in_specs, out_specs=out_specs, check_vma=False)
```

profile of v0, /device:TPU:0, one launch (start us, length us, event | category | flops | bytes accessed | tf_op | source)
XLA Modules:
  0.0 551.2 jit_solution(2232420375245703278)
XLA Ops:
  6.5 0.0 copy-start.5
  6.5 0.0 copy-start.6
  6.5 0.0 all-gather.8.cloned.1.call-start
  6.6 0.7 all-gather.8.cloned.1.call-update
  7.3 0.0 all-gather.12.cloned.1.call-start
  7.3 0.7 all-gather.12.cloned.1.call-update
  8.0 0.0 all-gather.10.cloned.1.call-start
  8.1 0.7 all-gather.10.cloned.1.call-update
  8.8 0.0 all-gather.16.cloned.1.call-start
  8.8 0.5 all-gather.16.cloned.1.call-update
  9.3 0.0 all-gather.14.cloned.1.call-start
  9.4 0.0 copy-done.5
  9.4 0.0 copy-done.6
  9.4 0.0 copy-done.3
  9.5 0.0 copy-done.4
  9.6 49.0 %all-gather.8.cloned.1.call-done = bf16[512,4096]{1,0:T(8,128)(2,1)} async-done(((bf16[512,512]{1,0:T(8,128)(2,1)}), bf16[512,4096]{1,0:T(8,128)(2,1)}) %all-gather.8.cloned.1.call-update) | async-done | bytes 4194320 | tf_op jit(solution)/shard_map/all_gather | solution.py:28
  58.6 3.1 fusion
  61.7 85.1 %all-gather.12.cloned.1.call-done = bf16[2,4096,512]{2,1,0:T(8,128)(2,1)} async-done(((bf16[2,1024,512]{2,1,0:T(8,128)(2,1)}), bf16[2,4096,512]{2,1,0:T(8,128)(2,1)}) %all-gather.12.cloned.1.call-update) | async-done | bytes 8388624 | tf_op jit(solution)/shard_map/all_gather | solution.py:23
  146.7 6.0 %fusion.21 = f32[512,512]{1,0:T(8,128)S(1)} fusion(bf16[2,4096,512]{2,1,0:T(8,128)(2,1)} %all-gather.12.cloned.1.call-done, bf16[512,4096]{1,0:T(8,128)(2,1)} %all-gather.8.cloned.1.call-done, f32[4096]{0:T(1024)S(1)} %bitcast.122, f32[512]{0:T(512)S(1)} %add_rsqrt_fusion.5), kind=kOutput, calls=%fused_computation.35 | convolution fusion | flops 2156658688 | bytes 9455616 | tf_op jit(solution)/shard_map/dot_general | solution.py:36
  152.7 0.0 copy-start.7
  152.7 83.4 %all-gather.10.cloned.1.call-done = bf16[2,4096,512]{2,1,0:T(8,128)(2,1)} async-done(((bf16[2,1024,512]{2,1,0:T(8,128)(2,1)}), bf16[2,4096,512]{2,1,0:T(8,128)(2,1)}) %all-gather.10.cloned.1.call-update) | async-done | bytes 8388624 | tf_op jit(solution)/shard_map/all_gather | solution.py:22
  236.1 5.8 %fusion.23 = bf16[512,512]{1,0:T(8,128)(2,1)S(1)} fusion(f32[512,512]{1,0:T(8,128)S(1)} %fusion.21, bf16[2,4096,512]{2,1,0:T(8,128)(2,1)} %all-gather.10.cloned.1.call-done, bf16[512,4096]{1,0:T(8,128)(2,1)} %all-gather.8.cloned.1.call-done, f32[4096]{0:T(1024)S(1)} %bitcast.123, f32[512]{0:T(512)S(1)} %add_rsqrt_fusion.5), kind=kOutput, calls=%fused_computation.37 | convolution fusion | flops 2156396544 | bytes 9979904 | tf_op jit(solution)/shard_map/dot_general | solution.py:35
  242.0 3.4 collective-permute-start
  245.4 0.0 copy-done.7
  245.4 1.6 collective-permute-done
  246.9 0.2 maximum_convert_fusion
  247.1 0.0 copy-start.8
  247.1 5.0 fusion.101
  252.1 15.3 %all-reduce.1 = (f32[512]{0:T(512)S(1)}, f32[512]{0:T(512)S(1)}) all-reduce(f32[512]{0:T(512)S(1)} %get-tuple-element.8, f32[512]{0:T(512)S(1)} %get-tuple-element.7), channel_id=1, replica_groups=mesh['sp'=4,'tp'=8] {'tp'}, use_global_device_ids=true, to_apply=%region_4.0 | all-reduce | flops 1024 | bytes 8192 | tf_op jit(solution)/shard_map/psum | solution.py:46
  267.4 1.2 multiply_convert_fusion.1
  268.7 0.0 all-gather.14.cloned.1.call-update
  268.7 0.0 all-gather.18.cloned.1.call-start
  268.7 0.0 copy-done.8
  268.8 0.0 copy-start.2
  268.8 56.5 %all-gather.16.cloned.1.call-done = bf16[2,4096,512]{2,1,0:T(8,128)(2,1)} async-done(((bf16[2,1024,512]{2,1,0:T(8,128)(2,1)}), bf16[2,4096,512]{2,1,0:T(8,128)(2,1)}) %all-gather.16.cloned.1.call-update) | async-done | bytes 8388624 | tf_op jit(solution)/shard_map/all_gather | solution.py:24
  325.3 48.4 %all-gather.14.cloned.1.call-done = bf16[512,4096]{1,0:T(8,128)(2,1)} async-done(((bf16[512,512]{1,0:T(8,128)(2,1)}), bf16[512,4096]{1,0:T(8,128)(2,1)}) %all-gather.14.cloned.1.call-update) | async-done | bytes 4194320 | tf_op jit(solution)/shard_map/all_gather | solution.py:55
  373.7 5.8 %fusion.24 = bf16[512,512]{1,0:T(8,128)(2,1)S(1)} fusion(bf16[512,4096]{1,0:T(8,128)(2,1)} %all-gather.14.cloned.1.call-done, bf16[2,4096,512]{2,1,0:T(8,128)(2,1)} %all-gather.16.cloned.1.call-done), kind=kOutput, calls=%fused_computation.38 | convolution fusion | flops 2147745792 | bytes 8912896 | tf_op jit(solution)/shard_map/dot_general | solution.py:56
  379.5 0.2 fusion.30
  379.6 14.8 %psum.44 = f32[512]{0:T(512)S(1)} all-reduce(f32[512]{0:T(512)S(1)} %fusion.30), channel_id=1, replica_groups=mesh['sp'=4,'tp'=8] {'tp'}, use_global_device_ids=true, to_apply=%region_6.7 | all-reduce | flops 512 | bytes 4096 | tf_op jit(solution)/shard_map/psum | solution.py:60
  394.4 0.0 copy-done.2
  394.5 1.1 fusion.33
  395.5 0.0 all-gather.18.cloned.1.call-update
  395.5 0.2 all-gather.20.cloned.1.call-start
  395.8 44.7 %all-gather.18.cloned.1.call-done = bf16[512,4096]{1,0:T(8,128)(2,1)} async-done(((bf16[512,512]{1,0:T(8,128)(2,1)}), bf16[512,4096]{1,0:T(8,128)(2,1)}) %all-gather.18.cloned.1.call-update) | async-done | bytes 4194320 | tf_op jit(solution)/shard_map/all_gather | solution.py:28
  440.5 3.2 fusion.3
  443.7 0.2 copy-done.1
  443.9 5.0 fusion.19
  448.9 0.0 slice-done
  448.9 0.0 slice-done.1
  449.0 2.4 fusion.22
  451.4 3.4 collective-permute-start.1
  454.9 1.5 collective-permute-done.1
  456.4 0.2 maximum_convert_fusion.1
  456.5 5.0 fusion.100
  461.6 13.7 %all-reduce = (f32[512]{0:T(512)S(1)}, f32[512]{0:T(512)S(1)}) all-reduce(f32[512]{0:T(512)S(1)} %get-tuple-element.6, f32[512]{0:T(512)S(1)} %get-tuple-element.5), channel_id=1, replica_groups=mesh['sp'=4,'tp'=8] {'tp'}, use_global_device_ids=true, to_apply=%region_11.12 | all-reduce | flops 1024 | bytes 8192 | tf_op jit(solution)/shard_map/psum | solution.py:46
  475.3 1.3 multiply_convert_fusion
  476.6 0.0 all-gather.20.cloned.1.call-update
  476.6 0.0 copy-start
  476.6 45.9 %all-gather.20.cloned.1.call-done = bf16[512,4096]{1,0:T(8,128)(2,1)} async-done(((bf16[512,512]{1,0:T(8,128)(2,1)}), bf16[512,4096]{1,0:T(8,128)(2,1)}) %all-gather.20.cloned.1.call-update) | async-done | bytes 4194320 | tf_op jit(solution)/shard_map/all_gather | solution.py:55
  522.5 5.8 %fusion.25 = bf16[512,512]{1,0:T(8,128)(2,1)S(1)} fusion(bf16[512,4096]{1,0:T(8,128)(2,1)} %all-gather.20.cloned.1.call-done, bf16[2,4096,512]{2,1,0:T(8,128)(2,1)} %all-gather.16.cloned.1.call-done), kind=kOutput, calls=%fused_computation.39 | convolution fusion | flops 2147745792 | bytes 8912896 | tf_op jit(solution)/shard_map/dot_general | solution.py:56
  528.3 0.2 fusion.34
  528.5 14.8 %psum.47 = f32[512]{0:T(512)S(1)} all-reduce(f32[512]{0:T(512)S(1)} %fusion.34), channel_id=1, replica_groups=mesh['sp'=4,'tp'=8] {'tp'}, use_global_device_ids=true, to_apply=%region_13.14 | all-reduce | flops 512 | bytes 4096 | tf_op jit(solution)/shard_map/psum | solution.py:60
  543.3 0.0 copy-done
  543.3 1.1 fusion.37
  (23 shorter events, 0.3 us)
Async XLA Ops:
  6.5 2.8 copy-start.5
  6.5 2.9 copy-start.6
  6.5 2.9 copy-start.3
  6.5 3.0 copy-start.4
  6.5 52.0 %all-gather.8.cloned.1.call-start = ((), (), s32[]{:S(2)}) async-start(), calls=%async_computation | async-start | bytes 4718592 | tf_op jit(solution)/shard_map/all_gather | solution.py:28
  7.3 139.5 %all-gather.12.cloned.1.call-start = ((), (), s32[]{:S(2)}) async-start(), calls=%async_computation.2 | async-start | bytes 10485760 | tf_op jit(solution)/shard_map/all_gather | solution.py:23
  8.0 228.1 %all-gather.10.cloned.1.call-start = ((), (), s32[]{:S(2)}) async-start(), calls=%async_computation.1 | async-start | bytes 10485760 | tf_op jit(solution)/shard_map/all_gather | solution.py:22
  8.8 316.6 %all-gather.16.cloned.1.call-start = ((), (), s32[]{:S(2)}) async-start(), calls=%async_computation.4 | async-start | bytes 10485760 | tf_op jit(solution)/shard_map/all_gather | solution.py:24
  9.3 364.3 %all-gather.14.cloned.1.call-start = ((), (), s32[]{:S(2)}) async-start(), calls=%async_computation.3 | async-start | bytes 4718592 | tf_op jit(solution)/shard_map/all_gather | solution.py:55
  152.7 92.6 %copy-start.7 = (f32[2,512]{1,0:T(2,128)S(1)}, f32[2,512]{1,0:T(2,128)}, u32[]{:S(2)}) copy-start(f32[2,512]{1,0:T(2,128)} %param.16) | copy-start | bytes 12292
  242.0 5.0 collective-permute-start
  247.1 21.7 %copy-start.8 = (f32[2,512]{1,0:T(2,128)S(1)}, f32[2,512]{1,0:T(2,128)}, u32[]{:S(2)}) copy-start(f32[2,512]{1,0:T(2,128)} %param.19) | copy-start | bytes 12292
  268.7 171.8 %all-gather.18.cloned.1.call-start = ((), (), s32[]{:S(2)}) async-start(), calls=%async_computation.5 | async-start | bytes 4718592 | tf_op jit(solution)/shard_map/all_gather | solution.py:28
  268.8 125.7 %copy-start.2 = (bf16[512,512]{1,0:T(8,128)(2,1)S(1)}, bf16[512,512]{1,0:T(8,128)(2,1)}, u32[]{:S(2)}) copy-start(bf16[512,512]{1,0:T(8,128)(2,1)} %param.10) | copy-start | bytes 1572868
  395.5 127.0 %all-gather.20.cloned.1.call-start = ((), (), s32[]{:S(2)}) async-start(), calls=%async_computation.6 | async-start | bytes 4718592 | tf_op jit(solution)/shard_map/all_gather | solution.py:55
  440.5 3.4 copy-start.1
  440.5 8.5 %slice-start = ((s8[8388608]{0:T(1024)(128)(4,1)}), s8[4194304]{0:T(1024)(128)(4,1)S(1)}, s32[]{:S(2)}) async-start(s8[8388608]{0:T(1024)(128)(4,1)} %bitcast.194), calls=%async_computation.7 | async-start | bytes 8388608
  443.9 5.0 slice-start.1
  451.4 5.0 collective-permute-start.1
  476.6 66.7 %copy-start = (bf16[512,512]{1,0:T(8,128)(2,1)S(1)}, bf16[512,512]{1,0:T(8,128)(2,1)}, u32[]{:S(2)}) copy-start(bf16[512,512]{1,0:T(8,128)(2,1)} %fusion.33) | copy-start | bytes 1572868
Sparse Core Ops, SparseCore 0:
  9.0 49.5 all-gather.7
  60.4 86.2 all-gather.11
  148.6 87.4 all-gather.9
  237.8 87.4 all-gather.15
  326.8 46.8 all-gather.13
  395.7 44.7 all-gather.17
  476.7 45.7 all-gather.19
where the time goes:
time: 551 us
  waiting for transfers between devices  419 us (76%)
  blocking collectives  58.7 us (11%)
  matrix products  30.8 us (6%)
  other arithmetic  21.7 us (4%)
  between operations  13.8 us (3%)
  starting transfers between devices  7.2 us (1%)
    all_gather x2, waiting for transfers between devices, shards(): whole_mixed = lax.all_gather(mixed, 'tp', axis=1, tiled=True)  94.2 us
    all_gather x2, waiting for transfers between devices, shards(): gathered = lax.all_gather(stream, 'tp', axis=1, tiled=True)  93.7 us
    all_gather x1, waiting for transfers between devices, shards(): lax.all_gather(w_gate, 'sp', axis=1, tiled=True)  85.1 us
    all_gather x1, waiting for transfers between devices, shards(): lax.all_gather(w_value, 'sp', axis=1, tiled=True)  83.4 us
    all_gather x1, waiting for transfers between devices, shards(): lax.all_gather(w_out, 'sp', axis=1, tiled=True)  56.5 us
    psum x2, blocking collectives, shards(): total = lax.psum(jnp.sum(branch * branch, axis=-1), 'tp')  29.6 us
    psum x2, blocking collectives, shards(): lax.psum((jnp.sum(filtered, axis=-1), jnp.sum(filtered * filtered, axis=-...  29.1 us
    dot_general x2, matrix products, shards(): jnp.dot(whole_mixed, out_block, preferred_element_type=jnp.float32)  11.6 us
  transfers between devices with their start and end apart: 9, of which 9 were waited for; matrix products, arithmetic and copies ran while one was open for 4% of the time, Pallas kernels for 0%

commit v1 on v0

--- a/solution.py
+++ b/solution.py
@@ -2,6 +2,7 @@
 import jax.numpy as jnp
 from jax import lax
 from jax.sharding import PartitionSpec as P
+from jax.lax import all_gather
 
 
 def passed_along(value, axis, steps):
@@ -18,10 +19,16 @@
     channel_count = conv_taps.shape[2] * lax.axis_size("tp")
     model_width = tokens.shape[1] * lax.axis_size("tp")
     local_rows = tokens.shape[0]
+
+    def sites_note(row_data, a_name):
+        far_arr = all_gather(row_data, a_name)
+        everything = jnp.concatenate(far_arr, axis=1)
+        return everything
+
     every_value, every_gate, every_out = (
         lax.all_gather(w_value, "sp", axis=1, tiled=True),
         lax.all_gather(w_gate, "sp", axis=1, tiled=True),
-        lax.all_gather(w_out, "sp", axis=1, tiled=True),
+        sites_note(w_out, "sp"),
     )
     stream = tokens
     for layer_index in range(layer_count):

time: 551 us -> 551 us (level)
  waiting for transfers between devices: 419 us -> 413 us
  local copies, waits for them, and re-layouts: 0.46 us -> 6.22 us
    slice x0 -> x1, local copies, waits for them, and re-layouts: none -> 5.76 us  [shards(): out_block = every_out[layer_index]]
    all_gather x2, waiting for transfers between devices: 94.2 us -> 88.5 us  [shards(): whole_mixed = lax.all_gather(mixed, 'tp', axis=1, tiled=True)]
  transfers between devices with their start and end apart: 9 -> 9, of which waited for: 9 -> 9; matrix products, arithmetic and copies ran while one was open for 4% -> 5% of each run, Pallas kernels for 0% -> 0%
where the time goes in v1:
time: 551 us
  waiting for transfers between devices  413 us (75%)
  blocking collectives  58.7 us (11%)
  matrix products  30.9 us (6%)
  other arithmetic  21.6 us (4%)
  between operations  13.8 us (3%)
  starting transfers between devices  7.2 us (1%)
  local copies, waits for them, and re-layouts  6.22 us (1%)
    all_gather x2, waiting for transfers between devices, shards(): gathered = lax.all_gather(stream, 'tp', axis=1, tiled=True)  93.7 us
    all_gather x2, waiting for transfers between devices, shards(): whole_mixed = lax.all_gather(mixed, 'tp', axis=1, tiled=True)  88.5 us
    all_gather x1, waiting for transfers between devices, shards(): lax.all_gather(w_gate, 'sp', axis=1, tiled=True)  85.1 us
    all_gather x1, waiting for transfers between devices, shards(): lax.all_gather(w_value, 'sp', axis=1, tiled=True)  83.4 us
    all_gather x1, waiting for transfers between devices, sites_note(): far_arr = all_gather(row_data, a_name)  56.5 us
    psum x2, blocking collectives, shards(): total = lax.psum(jnp.sum(branch * branch, axis=-1), 'tp')  29.6 us
    psum x2, blocking collectives, shards(): lax.psum((jnp.sum(filtered, axis=-1), jnp.sum(filtered * filtered, axis=-...  29 us
    dot_general x2, matrix products, shards(): jnp.dot(whole_mixed, out_block, preferred_element_type=jnp.float32)  11.7 us
  transfers between devices with their start and end apart: 9, of which 9 were waited for; matrix products, arithmetic and copies ran while one was open for 5% of the time, Pallas kernels for 0%

profile of v1, /device:TPU:0, one launch (start us, length us, event | category | flops | bytes accessed | tf_op | source)
XLA Modules:
  0.0 551.2 jit_solution(2187730576667447221)
XLA Ops:
  6.5 0.0 copy-start.5
  6.5 0.0 copy-start.6
  6.5 0.0 copy-start.3
  6.5 0.0 all-gather.9.cloned.1.call-start
  6.6 0.7 all-gather.9.cloned.1.call-update
  7.3 0.0 all-gather.13.cloned.1.call-start
  7.3 0.7 all-gather.13.cloned.1.call-update
  8.0 0.0 all-gather.11.cloned.1.call-start
  8.1 0.7 all-gather.11.cloned.1.call-update
  8.8 0.0 all-gather.21.cloned.1.call-start
  8.8 0.5 all-gather.21.cloned.1.call-update
  9.3 0.0 all-gather.15.cloned.1.call-start
  9.4 0.0 copy-done.5
  9.4 0.0 copy-done.6
  9.4 0.0 copy-done.3
  9.5 0.0 copy-done.4
  9.6 49.0 %all-gather.9.cloned.1.call-done = bf16[512,4096]{1,0:T(8,128)(2,1)} async-done(((bf16[512,512]{1,0:T(8,128)(2,1)}), bf16[512,4096]{1,0:T(8,128)(2,1)}) %all-gather.9.cloned.1.call-update) | async-done | bytes 4194320 | tf_op jit(solution)/shard_map/all_gather | solution.py:35
  58.6 3.1 fusion
  61.7 85.1 %all-gather.13.cloned.1.call-done = bf16[2,4096,512]{2,1,0:T(8,128)(2,1)} async-done(((bf16[2,1024,512]{2,1,0:T(8,128)(2,1)}), bf16[2,4096,512]{2,1,0:T(8,128)(2,1)}) %all-gather.13.cloned.1.call-update) | async-done | bytes 8388624 | tf_op jit(solution)/shard_map/all_gather | solution.py:30
  146.7 6.0 %fusion.19 = f32[512,512]{1,0:T(8,128)S(1)} fusion(bf16[2,4096,512]{2,1,0:T(8,128)(2,1)} %all-gather.13.cloned.1.call-done, bf16[512,4096]{1,0:T(8,128)(2,1)} %all-gather.9.cloned.1.call-done, f32[4096]{0:T(1024)S(1)} %bitcast.122, f32[512]{0:T(512)S(1)} %add_rsqrt_fusion.5), kind=kOutput, calls=%fused_computation.31 | convolution fusion | flops 2156658688 | bytes 9455616 | tf_op jit(solution)/shard_map/dot_general | solution.py:43
  152.7 0.0 copy-start.7
  152.7 83.4 %all-gather.11.cloned.1.call-done = bf16[2,4096,512]{2,1,0:T(8,128)(2,1)} async-done(((bf16[2,1024,512]{2,1,0:T(8,128)(2,1)}), bf16[2,4096,512]{2,1,0:T(8,128)(2,1)}) %all-gather.11.cloned.1.call-update) | async-done | bytes 8388624 | tf_op jit(solution)/shard_map/all_gather | solution.py:29
  236.1 5.8 %fusion.21 = bf16[512,512]{1,0:T(8,128)(2,1)S(1)} fusion(f32[512,512]{1,0:T(8,128)S(1)} %fusion.19, bf16[2,4096,512]{2,1,0:T(8,128)(2,1)} %all-gather.11.cloned.1.call-done, bf16[512,4096]{1,0:T(8,128)(2,1)} %all-gather.9.cloned.1.call-done, f32[4096]{0:T(1024)S(1)} %bitcast.123, f32[512]{0:T(512)S(1)} %add_rsqrt_fusion.5), kind=kOutput, calls=%fused_computation.33 | convolution fusion | flops 2156396544 | bytes 9979904 | tf_op jit(solution)/shard_map/dot_general | solution.py:42
  242.0 3.4 collective-permute-start
  245.4 0.0 copy-done.7
  245.4 1.6 collective-permute-done
  246.9 0.2 maximum_convert_fusion
  247.1 0.0 copy-start.8
  247.1 5.0 fusion.97
  252.1 15.3 %all-reduce.1 = (f32[512]{0:T(512)S(1)}, f32[512]{0:T(512)S(1)}) all-reduce(f32[512]{0:T(512)S(1)} %get-tuple-element.8, f32[512]{0:T(512)S(1)} %get-tuple-element.7), channel_id=1, replica_groups=mesh['sp'=4,'tp'=8] {'tp'}, use_global_device_ids=true, to_apply=%region_4.0 | all-reduce | flops 1024 | bytes 8192 | tf_op jit(solution)/shard_map/psum | solution.py:53
  267.4 1.2 multiply_convert_fusion.1
  268.7 0.0 all-gather.15.cloned.1.call-update
  268.7 0.0 all-gather.17.cloned.1.call-start
  268.7 0.0 copy-done.8
  268.8 56.5 %all-gather.21.cloned.1.call-done = bf16[8,1024,512]{2,1,0:T(8,128)(2,1)} async-done(((bf16[2,1024,512]{2,1,0:T(8,128)(2,1)}), bf16[8,1024,512]{2,1,0:T(8,128)(2,1)}) %all-gather.21.cloned.1.call-update) | async-done | bytes 8388624 | tf_op jit(solution)/shard_map/all_gather | solution.py:24
  325.3 5.8 %fusion.100 = (bf16[1,4,1024,512]{3,2,0,1:T(8,128)(2,1)}, bf16[1,4,1024,512]{3,2,0,1:T(8,128)(2,1)}) fusion(bf16[2,4,1024,512]{3,2,0,1:T(8,128)(2,1)} %bitcast.117), kind=kLoop, calls=%fused_computation.184 | loop fusion | bytes 16777216 | tf_op jit(solution)/shard_map/slice | solution.py:41
  331.1 42.6 %all-gather.15.cloned.1.call-done = bf16[512,4096]{1,0:T(8,128)(2,1)} async-done(((bf16[512,512]{1,0:T(8,128)(2,1)}), bf16[512,4096]{1,0:T(8,128)(2,1)}) %all-gather.15.cloned.1.call-update) | async-done | bytes 4194320 | tf_op jit(solution)/shard_map/all_gather | solution.py:62
  373.7 5.8 %convolution_convert_fusion.1 = bf16[512,512]{1,0:T(8,128)(2,1)S(1)} fusion(bf16[512,4096]{1,0:T(8,128)(2,1)} %all-gather.15.cloned.1.call-done, bf16[4096,512]{1,0:T(8,128)(2,1)} %bitcast.119), kind=kOutput, calls=%fused_computation.35 | convolution fusion | flops 2147745792 | bytes 8912896 | tf_op jit(solution)/shard_map/dot_general | solution.py:63
  379.5 0.2 fusion.26
  379.7 14.8 %psum.44 = f32[512]{0:T(512)S(1)} all-reduce(f32[512]{0:T(512)S(1)} %fusion.26), channel_id=1, replica_groups=mesh['sp'=4,'tp'=8] {'tp'}, use_global_device_ids=true, to_apply=%region_6.7 | all-reduce | flops 512 | bytes 4096 | tf_op jit(solution)/shard_map/psum | solution.py:67
  394.5 0.0 copy-done.2
  394.5 1.1 fusion.29
  395.6 0.0 all-gather.17.cloned.1.call-update
  395.6 0.2 all-gather.19.cloned.1.call-start
  395.8 44.7 %all-gather.17.cloned.1.call-done = bf16[512,4096]{1,0:T(8,128)(2,1)} async-done(((bf16[512,512]{1,0:T(8,128)(2,1)}), bf16[512,4096]{1,0:T(8,128)(2,1)}) %all-gather.17.cloned.1.call-update) | async-done | bytes 4194320 | tf_op jit(solution)/shard_map/all_gather | solution.py:35
  440.5 3.2 fusion.3
  443.8 0.2 copy-done.1
  444.0 5.0 fusion.17
  449.0 0.0 slice-done
  449.0 0.0 slice-done.1
  449.0 2.4 fusion.20
  451.4 3.4 collective-permute-start.1
  454.9 1.5 collective-permute-done.1
  456.4 0.2 maximum_convert_fusion.1
  456.5 5.0 fusion.96
  461.5 13.7 %all-reduce = (f32[512]{0:T(512)S(1)}, f32[512]{0:T(512)S(1)}) all-reduce(f32[512]{0:T(512)S(1)} %get-tuple-element.6, f32[512]{0:T(512)S(1)} %get-tuple-element.5), channel_id=1, replica_groups=mesh['sp'=4,'tp'=8] {'tp'}, use_global_device_ids=true, to_apply=%region_11.12 | all-reduce | flops 1024 | bytes 8192 | tf_op jit(solution)/shard_map/psum | solution.py:53
  475.3 1.2 multiply_convert_fusion
  476.5 0.0 all-gather.19.cloned.1.call-update
  476.5 45.9 %all-gather.19.cloned.1.call-done = bf16[512,4096]{1,0:T(8,128)(2,1)} async-done(((bf16[512,512]{1,0:T(8,128)(2,1)}), bf16[512,4096]{1,0:T(8,128)(2,1)}) %all-gather.19.cloned.1.call-update) | async-done | bytes 4194320 | tf_op jit(solution)/shard_map/all_gather | solution.py:62
  522.4 5.8 %convolution_convert_fusion = bf16[512,512]{1,0:T(8,128)(2,1)S(1)} fusion(bf16[512,4096]{1,0:T(8,128)(2,1)} %all-gather.19.cloned.1.call-done, bf16[4096,512]{1,0:T(8,128)(2,1)} %bitcast.118), kind=kOutput, calls=%fused_computation.34 | convolution fusion | flops 2147745792 | bytes 8912896 | tf_op jit(solution)/shard_map/dot_general | solution.py:63
  528.3 0.2 fusion.30
  528.4 14.8 %psum.47 = f32[512]{0:T(512)S(1)} all-reduce(f32[512]{0:T(512)S(1)} %fusion.30), channel_id=1, replica_groups=mesh['sp'=4,'tp'=8] {'tp'}, use_global_device_ids=true, to_apply=%region_13.14 | all-reduce | flops 512 | bytes 4096 | tf_op jit(solution)/shard_map/psum | solution.py:67
  543.3 0.0 copy-done
  543.3 1.1 fusion.33
  (24 shorter events, 0.3 us)
Async XLA Ops:
  6.5 2.8 copy-start.5
  6.5 2.9 copy-start.6
  6.5 2.9 copy-start.3
  6.5 3.0 copy-start.4
  6.5 52.0 %all-gather.9.cloned.1.call-start = ((), (), s32[]{:S(2)}) async-start(), calls=%async_computation | async-start | bytes 4718592 | tf_op jit(solution)/shard_map/all_gather | solution.py:35
  7.3 139.5 %all-gather.13.cloned.1.call-start = ((), (), s32[]{:S(2)}) async-start(), calls=%async_computation.2 | async-start | bytes 10485760 | tf_op jit(solution)/shard_map/all_gather | solution.py:30
  8.0 228.1 %all-gather.11.cloned.1.call-start = ((), (), s32[]{:S(2)}) async-start(), calls=%async_computation.1 | async-start | bytes 10485760 | tf_op jit(solution)/shard_map/all_gather | solution.py:29
  8.8 316.6 %all-gather.21.cloned.1.call-start = ((), (), s32[]{:S(2)}) async-start(), calls=%async_computation.6 | async-start | bytes 10485760 | tf_op jit(solution)/shard_map/all_gather | solution.py:24
  9.3 364.3 %all-gather.15.cloned.1.call-start = ((), (), s32[]{:S(2)}) async-start(), calls=%async_computation.3 | async-start | bytes 4718592 | tf_op jit(solution)/shard_map/all_gather | solution.py:62
  152.7 92.6 %copy-start.7 = (f32[2,512]{1,0:T(2,128)S(1)}, f32[2,512]{1,0:T(2,128)}, u32[]{:S(2)}) copy-start(f32[2,512]{1,0:T(2,128)} %param.17) | copy-start | bytes 12292
  242.0 5.0 collective-permute-start
  247.1 21.6 %copy-start.8 = (f32[2,512]{1,0:T(2,128)S(1)}, f32[2,512]{1,0:T(2,128)}, u32[]{:S(2)}) copy-start(f32[2,512]{1,0:T(2,128)} %param.19) | copy-start | bytes 12292
  268.7 171.8 %all-gather.17.cloned.1.call-start = ((), (), s32[]{:S(2)}) async-start(), calls=%async_computation.4 | async-start | bytes 4718592 | tf_op jit(solution)/shard_map/all_gather | solution.py:35
  373.7 20.8 %copy-start.2 = (bf16[512,512]{1,0:T(8,128)(2,1)S(1)}, bf16[512,512]{1,0:T(8,128)(2,1)}, u32[]{:S(2)}) copy-start(bf16[512,512]{1,0:T(8,128)(2,1)} %param.10) | copy-start | bytes 1572868
  395.6 126.9 %all-gather.19.cloned.1.call-start = ((), (), s32[]{:S(2)}) async-start(), calls=%async_computation.5 | async-start | bytes 4718592 | tf_op jit(solution)/shard_map/all_gather | solution.py:62
  440.5 3.4 copy-start.1
  440.5 8.5 %slice-start = ((s8[8388608]{0:T(1024)(128)(4,1)}), s8[4194304]{0:T(1024)(128)(4,1)S(1)}, s32[]{:S(2)}) async-start(s8[8388608]{0:T(1024)(128)(4,1)} %bitcast.194), calls=%async_computation.7 | async-start | bytes 8388608
  444.0 5.0 slice-start.1
  451.4 5.0 collective-permute-start.1
  522.4 20.8 %copy-start = (bf16[512,512]{1,0:T(8,128)(2,1)S(1)}, bf16[512,512]{1,0:T(8,128)(2,1)}, u32[]{:S(2)}) copy-start(bf16[512,512]{1,0:T(8,128)(2,1)} %fusion.29) | copy-start | bytes 1572868
Sparse Core Ops, SparseCore 0:
  9.0 49.5 all-gather.8
  60.4 86.2 all-gather.12
  148.6 87.4 all-gather.10
  237.8 87.4 all-gather.20
  326.8 46.8 all-gather.14
  395.7 44.7 all-gather.16
  476.7 45.7 all-gather.18
